TPU v7x, 512 devices: a whole 4x4x16 slice. The times are simulated.
512 devices in a mesh: ep: 32 (over z, core), tp: 16 (over y, x).
Axes of the slice: x: 4, y: 4, z: 16, core: 2. Of those that a mesh axis runs over, the one named last changes fastest.
Arguments:
- queries: bfloat16 [16384, 2048], P('ep', 'tp'), may hold values from -220 to 220
- keys: bfloat16 [16384, 2048], P('ep', 'tp'), may hold values from -6 to 6
- values: bfloat16 [16384, 2048], P('ep', 'tp'), may hold values from -6 to 6
- log_gate_sums: float32 [16384, 16], P(None, 'tp'), may hold values from -16384 to 0, as said below
- mixer_weight: bfloat16 [2048, 2048], P('tp'), may hold values from -2.5 to 2.5
- moe_rows: bfloat16 [6144, 2048], P('ep'), may hold values from -6 to 6
- route_ids: int32 [6144, 2], P('ep'), may hold values from 0 to 31, all different within a row; in each aligned block of 192 rows (0 to 191, 192 to 383, ...) at most 18 rows name the same one
- group_gate: float32 [6144], P('ep'), may hold values from 0.25 to 1
- inner_gate: float32 [6144, 2], P('ep'), may hold values from 0.2 to 1
- norm_gain: float32 [2048], replicated, may hold values from 0.1 to 1.9
- gate_weight: bfloat16 [32, 2048, 4096], P('ep', None, 'tp'), may hold values from -0.125 to 0.125
- up_weight: bfloat16 [32, 2048, 4096], P('ep', None, 'tp'), may hold values from -0.125 to 0.125
- down_weight: bfloat16 [32, 4096, 2048], P('ep', 'tp'), may hold values from -0.09375 to 0.09375
Outputs:
- mixer_out: bfloat16 [16384, 2048], P('ep', 'tp')
- moe_out: bfloat16 [6144, 2048], P('ep', 'tp')
Inputs may be any that keep to these rules, and one draw needn't show every extreme that they name: `route_ids`: each row names 2 different experts; among the rows of one index of ep no expert is named more than 18 times, a bound that some block reaches. `log_gate_sums`: never rising along the positions of a head.
All inputs are finite; a program needn't handle non-finite values.
Results may differ from a plain program's by a relative error of at most 0.015.
Values may be sent and summed in bfloat16 or wider, within the bound.
No kernel may reach another device: no remote copies, remote signals or barrier semaphores. Data moves between devices by JAX's collectives and lax.ppermute only.
A program may use at most 64 MiB of HBM per device.

v0:
```python
import jax
import jax.numpy as jnp
from jax import lax
from jax.sharding import PartitionSpec as P

LOW_SCORE = -1e30
NORM_EPS = 1e-06


def sent_together(arrays, axis, dim, along):
    widths = [a.shape[along] for a in arrays]
    both = jnp.concatenate(arrays, axis=along)
    out = lax.all_gather(both, axis, axis=dim, tiled=True)
    return tuple(jnp.split(out, [sum(widths[:k]) for k in range(1, len(widths))], axis=along))


def cut_along(x, dim, count):
    before, after = (x.shape[:dim], x.shape[dim + 1 :])
    return jnp.moveaxis(x.reshape(*before, count, -1, *after), dim, 0)


def sum_at_owner(x, axis, dim):
    tiles = cut_along(x, dim, lax.axis_size(axis))
    arrived = lax.all_to_all(tiles, axis, split_axis=0, concat_axis=0, tiled=True)
    return arrived.astype(jnp.float32).sum(axis=0)


def from_everyone(x, axis):
    copies = jnp.broadcast_to(x, (lax.axis_size(axis), *x.shape))
    return lax.all_to_all(copies, axis, split_axis=0, concat_axis=0, tiled=True)


def laid_out(tiles, dim):
    dims = list(tiles.shape[1:])
    dims[dim] *= tiles.shape[0]
    return jnp.moveaxis(tiles, 0, dim).reshape(dims)


def collect(x, axis, dim):
    tiles = from_everyone(x, axis)
    return laid_out(tiles, dim)


def attend_block(
    running,
    queries_here,
    query_gates,
    key_rows,
    value_rows,
    key_gates,
    query_pos,
    key_pos,
    inv_root,
):
    running_max, weight_sum, weighted = running
    scores = (
        jnp.einsum("qhd,khd->qhk", queries_here, key_rows, preferred_element_type=jnp.float32)
        * inv_root
    )
    scores = scores + query_gates[:, :, None] - key_gates.T[None, :, :]
    allowed = (key_pos[None, :] <= query_pos[:, None])[:, None, :]
    scores = jnp.where(allowed, scores, LOW_SCORE)
    new_max = jnp.maximum(running_max, jnp.max(scores, axis=2))
    shrink = jnp.exp(running_max - new_max)
    weights_now = jnp.where(allowed, jnp.exp(scores - new_max[:, :, None]), 0.0)
    weight_sum = weight_sum * shrink + jnp.sum(weights_now, axis=2)
    weighted = weighted * shrink[:, :, None] + jnp.einsum(
        "qhk,khd->qhd",
        weights_now.astype(jnp.bfloat16),
        value_rows,
        preferred_element_type=jnp.float32,
    )
    return (new_max, weight_sum, weighted)


def body(
    queries,
    keys,
    values,
    log_gate_sums,
    mixer_weight,
    moe_rows,
    route_ids,
    group_gate,
    inner_gate,
    norm_gain,
    gate_weight,
    up_weight,
    down_weight,
):
    row_count = queries.shape[0]
    heads_here = log_gate_sums.shape[1]
    head_width = queries.shape[1] // heads_here
    inv_root = head_width ** (-0.5)
    row_offset = lax.axis_index("ep") * row_count
    query_pos = row_offset + jnp.arange(row_count, dtype=jnp.int32)
    queries_here = queries.reshape(row_count, heads_here, head_width)
    query_gates = lax.dynamic_slice_in_dim(log_gate_sums, row_offset, row_count, 0)
    last_query = row_offset + row_count - 1
    start_state = (
        jnp.full((row_count, heads_here), LOW_SCORE, jnp.float32),
        jnp.zeros((row_count, heads_here), jnp.float32),
        jnp.zeros((row_count, heads_here, head_width), jnp.float32),
    )
    key_piece, value_piece = sent_together((keys, values), "ep", 0, 1)
    piece_rows = key_piece.shape[0]

    def key_step(block_index, partial_state):
        key_offset = block_index * row_count
        key_rows = lax.dynamic_slice_in_dim(key_piece, key_offset, row_count, 0).reshape(
            row_count, heads_here, head_width
        )
        value_rows = lax.dynamic_slice_in_dim(value_piece, key_offset, row_count, 0).reshape(
            row_count, heads_here, head_width
        )
        key_gates = lax.dynamic_slice_in_dim(log_gate_sums, key_offset, row_count, 0)
        key_pos = key_offset + jnp.arange(row_count, dtype=jnp.int32)

        def update(state_in):
            return attend_block(
                state_in,
                queries_here,
                query_gates,
                key_rows,
                value_rows,
                key_gates,
                query_pos,
                key_pos,
                inv_root,
            )

        def unchanged(state_in):
            return state_in

        return lax.cond(key_offset <= last_query, update, unchanged, partial_state)

    running_max, weight_sum, weighted = lax.fori_loop(
        0, piece_rows // row_count, key_step, start_state
    )
    attended = (
        (weighted / weight_sum[:, :, None])
        .astype(jnp.bfloat16)
        .reshape(row_count, heads_here * head_width)
    )
    partial_value = jnp.dot(attended, mixer_weight, preferred_element_type=jnp.float32).astype(
        jnp.bfloat16
    )
    partial_value = lax.optimization_barrier(partial_value).astype(jnp.float32)
    mixer_out = sum_at_owner(partial_value.astype(jnp.bfloat16), "tp", 1).astype(jnp.bfloat16)
    token_count = moe_rows.shape[0]
    top_count = route_ids.shape[1]
    model_width = moe_rows.shape[1]
    local_experts = gate_weight.shape[0]
    experts = lax.axis_size("ep") * local_experts
    capacity = 3 * token_count * top_count // (2 * experts)
    slot_count = experts * capacity
    rows_float = moe_rows.astype(jnp.float32)
    normed = (
        rows_float
        * lax.rsqrt(jnp.mean(rows_float * rows_float, axis=1, keepdims=True) + NORM_EPS)
        * norm_gain
    ).astype(jnp.bfloat16)
    route_weight = group_gate[:, None] * inner_gate / jnp.sum(inner_gate, axis=1, keepdims=True)
    onehot = (route_ids[:, :, None] == jnp.arange(experts, dtype=jnp.int32)[None, None, :]).astype(
        jnp.int32
    )
    onehot = onehot.reshape(token_count * top_count, experts)
    earlier_hits = jnp.cumsum(onehot, axis=0) - onehot
    slot_index = jnp.sum(earlier_hits * onehot, axis=1) + route_ids.reshape(-1) * capacity
    slot_hit = (slot_index[:, None] == jnp.arange(slot_count, dtype=jnp.int32)[None, :]).reshape(
        token_count, top_count, slot_count
    )
    dispatch = jnp.sum(slot_hit.astype(jnp.float32), axis=1).astype(jnp.bfloat16)
    combine = jnp.sum(jnp.where(slot_hit, route_weight[:, :, None], 0.0), axis=1)
    feature_cols = model_width // lax.axis_size("tp")
    own_features = lax.dynamic_slice_in_dim(
        normed, lax.axis_index("tp") * feature_cols, feature_cols, 1
    )
    outgoing = lax.dot_general(
        dispatch, own_features, (((0,), (0,)), ((), ())), preferred_element_type=jnp.float32
    ).astype(jnp.bfloat16)
    arrived = lax.all_to_all(outgoing, "ep", split_axis=0, concat_axis=0, tiled=True)
    sources = arrived.shape[0] // (local_experts * capacity)
    column_piece = collect(arrived, "tp", 1)
    piece_cols = column_piece.shape[1]
    piece_blocks = column_piece.reshape(sources, local_experts, capacity, piece_cols)
    gate_sum = jnp.einsum(
        "secd,edf->secf", piece_blocks, gate_weight, preferred_element_type=jnp.float32
    )
    up_sum = jnp.einsum(
        "secd,edf->secf", piece_blocks, up_weight, preferred_element_type=jnp.float32
    )
    hidden = (jax.nn.silu(gate_sum) * up_sum).astype(jnp.bfloat16)
    expert_part = jnp.einsum(
        "secf,efd->secd", hidden, down_weight, preferred_element_type=jnp.float32
    ).astype(jnp.bfloat16)
    expert_part = (
        lax.optimization_barrier(expert_part).astype(jnp.float32).reshape(slot_count, model_width)
    )
    expert_out = sum_at_owner(expert_part.astype(jnp.bfloat16), "tp", 1).astype(jnp.bfloat16)
    returned_rows = lax.all_to_all(expert_out, "ep", split_axis=0, concat_axis=0, tiled=True)
    moe_out = jnp.dot(
        combine, returned_rows.astype(jnp.float32), precision=lax.Precision.HIGHEST
    ).astype(jnp.bfloat16)
    return (mixer_out, moe_out)


def solution(mesh):
    return jax.shard_map(
        body,
        mesh=mesh,
        in_specs=(
            P("ep", "tp"),
            P("ep", "tp"),
            P("ep", "tp"),
            P(None, "tp"),
            P("tp", None),
            P("ep", None),
            P("ep", None),
            P("ep"),
            P("ep", None),
            P(),
            P("ep", None, "tp"),
            P("ep", None, "tp"),
            P("ep", "tp", None),
        ),
        out_specs=(P("ep", "tp"), P("ep", "tp")),
        check_vma=False,
    )
```

profile of v0, /device:TPU:481, one launch (start us, length us, event | category | flops | bytes accessed | tf_op | source)
XLA Modules:
  0.0 312.8 jit_solution(2155545839781961805)
XLA Ops:
  15.5 25.2 %all_to_all.39 = bf16[32,18,128]{2,1,0:T(8,128)(2,1)S(1)} all-to-all(bf16[32,18,128]{2,1,0:T(8,128)(2,1)S(1)} %all_to_all.26), channel_id=1, replica_groups=mesh['ep'=32,'tp'=16] {'ep'}, dimensions={0} | all-to-all | bytes 294912 | tf_op jit(solution)/shard_map/all_to_all | solution.py:182
  41.2 36.3 %all_to_all.40 = bf16[16,576,128]{2,1,0:T(8,128)(2,1)S(1)} all-to-all(bf16[16,576,128]{2,1,0:T(8,128)(2,1)S(1)} %broadcast_in_dim.58), channel_id=1, replica_groups=mesh['ep'=32,'tp'=16] {'tp'}, dimensions={0} | all-to-all | bytes 4718592 | tf_op jit(solution)/shard_map/all_to_all | solution.py:30
  90.3 4.0 %convert_element_type.87 = bf16[576,16,128]{2,1,0:T(8,128)(2,1)S(1)} reshape(bf16[32,1,18,2048]{3,2,0,1:T(8,128)(2,1)} %copy.55) | data formatting | bytes 4718592 | tf_op jit(solution)/shard_map/convert_element_type | solution.py:200
  96.4 3.7 %all-to-all-start.3 = ((bf16[16,576,128]{2,1,0:T(8,128)(2,1)}), bf16[16,576,128]{2,1,0:T(8,128)(2,1)S(1)}, u32[]{:S(2)}, u32[]{:S(2)}) async-start(bf16[16,576,128]{2,1,0:T(8,128)(2,1)} %copy.56), calls=%async_computation.3 | async-start | bytes 4718592 | tf_op jit(solution)/shard_map/all_to_all | solution.py:24
  101.4 26.4 %all-to-all-done.3 = bf16[16,576,128]{2,1,0:T(8,128)(2,1)S(1)} async-done(((bf16[16,576,128]{2,1,0:T(8,128)(2,1)}), bf16[16,576,128]{2,1,0:T(8,128)(2,1)S(1)}, u32[]{:S(2)}, u32[]{:S(2)}) %all-to-all-start.3) | async-done | bytes 2359328 | tf_op jit(solution)/shard_map/all_to_all | solution.py:24
  128.8 17.9 %all-to-all-start.4 = ((bf16[32,18,128]{2,1,0:T(8,128)(2,1)}), bf16[32,18,128]{2,1,0:T(8,128)(2,1)S(1)}, u32[]{:S(2)}, u32[]{:S(2)}) async-start(bf16[32,18,128]{2,1,0:T(8,128)(2,1)} %all_to_all.31), calls=%async_computation.4 | async-start | bytes 393216 | tf_op jit(solution)/shard_map/all_to_all | solution.py:201
  146.8 5.7 %fusion.42 = (bf16[16384,128]{1,0:T(8,128)(2,1)}, bf16[16384,128]{1,0:T(8,128)(2,1)}) fusion(bf16[16384,256]{1,0:T(8,128)(2,1)} %all-gather.2.cloned.1.call-done), kind=kLoop, calls=%fused_computation.71 | loop fusion | bytes 16777216 | tf_op jit(solution)/shard_map/split | solution.py:14
  152.6 118.1 %while.18 = (s32[]{:T(128)}, f32[512,1]{0,1:T(1,128)S(1)}, f32[512,1]{0,1:T(1,128)S(1)}, f32[512,1,128]{0,2,1:T(8,128)S(1)}, s32[]{:T(128)}, /*index=5*/bf16[163...) while((s32[]{:T(128)}, f32[512,1]{0,1:T(1,128)S(1)}, ...), condition=%wide.region_5.6_spmd.clone, body=%wide.region_0.5_spmd.clone.sunk | while | flops 138020864 | bytes 4127077 | solution.py:137
  152.6 3.7 %conditional.3 = ((f32[512,1]{0,1:T(1,128)S(1)}, f32[512,1]{0,1:T(1,128)S(1)}, f32[512,1,128]{0,2,1:T(8,128)S(1)})) conditional(s32[]{:T(128)} %convert_element_type.116, (f32[512,1]{0,1:T(1,128)S(1)}, f32[512,1]{0,1:T(1,128)S(1)}, f32[512,1,128]{0,2,1:T(8,128)S(1)}) %tuple.60, (s32[]{:T(128)}, s32[512]{0:T(512)S(1)}, s32[]{:T(128)}, ...), branch_computations={%region_1.0_spmd, %region_2.4_spmd} | conditional | flops 138020864 | bytes 4124758 | solution.py:135
  163.7 3.6 %conditional.3 = ((f32[512,1]{0,1:T(1,128)S(1)}, f32[512,1]{0,1:T(1,128)S(1)}, f32[512,1,128]{0,2,1:T(8,128)S(1)})) conditional(s32[]{:T(128)} %convert_element_type.116, (f32[512,1]{0,1:T(1,128)S(1)}, f32[512,1]{0,1:T(1,128)S(1)}, f32[512,1,128]{0,2,1:T(8,128)S(1)}) %tuple.60, (s32[]{:T(128)}, s32[512]{0:T(512)S(1)}, s32[]{:T(128)}, ...), branch_computations={%region_1.0_spmd, %region_2.4_spmd} | conditional | flops 138020864 | bytes 4124758 | solution.py:135
  171.1 3.6 %conditional.3 = ((f32[512,1]{0,1:T(1,128)S(1)}, f32[512,1]{0,1:T(1,128)S(1)}, f32[512,1,128]{0,2,1:T(8,128)S(1)})) conditional(s32[]{:T(128)} %convert_element_type.116, (f32[512,1]{0,1:T(1,128)S(1)}, f32[512,1]{0,1:T(1,128)S(1)}, f32[512,1,128]{0,2,1:T(8,128)S(1)}) %tuple.60, (s32[]{:T(128)}, s32[512]{0:T(512)S(1)}, s32[]{:T(128)}, ...), branch_computations={%region_1.0_spmd, %region_2.4_spmd} | conditional | flops 138020864 | bytes 4124758 | solution.py:135
  178.5 3.6 %conditional.3 = ((f32[512,1]{0,1:T(1,128)S(1)}, f32[512,1]{0,1:T(1,128)S(1)}, f32[512,1,128]{0,2,1:T(8,128)S(1)})) conditional(s32[]{:T(128)} %convert_element_type.116, (f32[512,1]{0,1:T(1,128)S(1)}, f32[512,1]{0,1:T(1,128)S(1)}, f32[512,1,128]{0,2,1:T(8,128)S(1)}) %tuple.60, (s32[]{:T(128)}, s32[512]{0:T(512)S(1)}, s32[]{:T(128)}, ...), branch_computations={%region_1.0_spmd, %region_2.4_spmd} | conditional | flops 138020864 | bytes 4124758 | solution.py:135
  185.9 3.6 %conditional.3 = ((f32[512,1]{0,1:T(1,128)S(1)}, f32[512,1]{0,1:T(1,128)S(1)}, f32[512,1,128]{0,2,1:T(8,128)S(1)})) conditional(s32[]{:T(128)} %convert_element_type.116, (f32[512,1]{0,1:T(1,128)S(1)}, f32[512,1]{0,1:T(1,128)S(1)}, f32[512,1,128]{0,2,1:T(8,128)S(1)}) %tuple.60, (s32[]{:T(128)}, s32[512]{0:T(512)S(1)}, s32[]{:T(128)}, ...), branch_computations={%region_1.0_spmd, %region_2.4_spmd} | conditional | flops 138020864 | bytes 4124758 | solution.py:135
  193.3 3.6 %conditional.3 = ((f32[512,1]{0,1:T(1,128)S(1)}, f32[512,1]{0,1:T(1,128)S(1)}, f32[512,1,128]{0,2,1:T(8,128)S(1)})) conditional(s32[]{:T(128)} %convert_element_type.116, (f32[512,1]{0,1:T(1,128)S(1)}, f32[512,1]{0,1:T(1,128)S(1)}, f32[512,1,128]{0,2,1:T(8,128)S(1)}) %tuple.60, (s32[]{:T(128)}, s32[512]{0:T(512)S(1)}, s32[]{:T(128)}, ...), branch_computations={%region_1.0_spmd, %region_2.4_spmd} | conditional | flops 138020864 | bytes 4124758 | solution.py:135
  200.6 3.6 %conditional.3 = ((f32[512,1]{0,1:T(1,128)S(1)}, f32[512,1]{0,1:T(1,128)S(1)}, f32[512,1,128]{0,2,1:T(8,128)S(1)})) conditional(s32[]{:T(128)} %convert_element_type.116, (f32[512,1]{0,1:T(1,128)S(1)}, f32[512,1]{0,1:T(1,128)S(1)}, f32[512,1,128]{0,2,1:T(8,128)S(1)}) %tuple.60, (s32[]{:T(128)}, s32[512]{0:T(512)S(1)}, s32[]{:T(128)}, ...), branch_computations={%region_1.0_spmd, %region_2.4_spmd} | conditional | flops 138020864 | bytes 4124758 | solution.py:135
  208.0 3.6 %conditional.3 = ((f32[512,1]{0,1:T(1,128)S(1)}, f32[512,1]{0,1:T(1,128)S(1)}, f32[512,1,128]{0,2,1:T(8,128)S(1)})) conditional(s32[]{:T(128)} %convert_element_type.116, (f32[512,1]{0,1:T(1,128)S(1)}, f32[512,1]{0,1:T(1,128)S(1)}, f32[512,1,128]{0,2,1:T(8,128)S(1)}) %tuple.60, (s32[]{:T(128)}, s32[512]{0:T(512)S(1)}, s32[]{:T(128)}, ...), branch_computations={%region_1.0_spmd, %region_2.4_spmd} | conditional | flops 138020864 | bytes 4124758 | solution.py:135
  215.4 3.6 %conditional.3 = ((f32[512,1]{0,1:T(1,128)S(1)}, f32[512,1]{0,1:T(1,128)S(1)}, f32[512,1,128]{0,2,1:T(8,128)S(1)})) conditional(s32[]{:T(128)} %convert_element_type.116, (f32[512,1]{0,1:T(1,128)S(1)}, f32[512,1]{0,1:T(1,128)S(1)}, f32[512,1,128]{0,2,1:T(8,128)S(1)}) %tuple.60, (s32[]{:T(128)}, s32[512]{0:T(512)S(1)}, s32[]{:T(128)}, ...), branch_computations={%region_1.0_spmd, %region_2.4_spmd} | conditional | flops 138020864 | bytes 4124758 | solution.py:135
  222.8 3.6 %conditional.3 = ((f32[512,1]{0,1:T(1,128)S(1)}, f32[512,1]{0,1:T(1,128)S(1)}, f32[512,1,128]{0,2,1:T(8,128)S(1)})) conditional(s32[]{:T(128)} %convert_element_type.116, (f32[512,1]{0,1:T(1,128)S(1)}, f32[512,1]{0,1:T(1,128)S(1)}, f32[512,1,128]{0,2,1:T(8,128)S(1)}) %tuple.60, (s32[]{:T(128)}, s32[512]{0:T(512)S(1)}, s32[]{:T(128)}, ...), branch_computations={%region_1.0_spmd, %region_2.4_spmd} | conditional | flops 138020864 | bytes 4124758 | solution.py:135
  230.1 3.6 %conditional.3 = ((f32[512,1]{0,1:T(1,128)S(1)}, f32[512,1]{0,1:T(1,128)S(1)}, f32[512,1,128]{0,2,1:T(8,128)S(1)})) conditional(s32[]{:T(128)} %convert_element_type.116, (f32[512,1]{0,1:T(1,128)S(1)}, f32[512,1]{0,1:T(1,128)S(1)}, f32[512,1,128]{0,2,1:T(8,128)S(1)}) %tuple.60, (s32[]{:T(128)}, s32[512]{0:T(512)S(1)}, s32[]{:T(128)}, ...), branch_computations={%region_1.0_spmd, %region_2.4_spmd} | conditional | flops 138020864 | bytes 4124758 | solution.py:135
  237.5 3.6 %conditional.3 = ((f32[512,1]{0,1:T(1,128)S(1)}, f32[512,1]{0,1:T(1,128)S(1)}, f32[512,1,128]{0,2,1:T(8,128)S(1)})) conditional(s32[]{:T(128)} %convert_element_type.116, (f32[512,1]{0,1:T(1,128)S(1)}, f32[512,1]{0,1:T(1,128)S(1)}, f32[512,1,128]{0,2,1:T(8,128)S(1)}) %tuple.60, (s32[]{:T(128)}, s32[512]{0:T(512)S(1)}, s32[]{:T(128)}, ...), branch_computations={%region_1.0_spmd, %region_2.4_spmd} | conditional | flops 138020864 | bytes 4124758 | solution.py:135
  244.9 3.6 %conditional.3 = ((f32[512,1]{0,1:T(1,128)S(1)}, f32[512,1]{0,1:T(1,128)S(1)}, f32[512,1,128]{0,2,1:T(8,128)S(1)})) conditional(s32[]{:T(128)} %convert_element_type.116, (f32[512,1]{0,1:T(1,128)S(1)}, f32[512,1]{0,1:T(1,128)S(1)}, f32[512,1,128]{0,2,1:T(8,128)S(1)}) %tuple.60, (s32[]{:T(128)}, s32[512]{0:T(512)S(1)}, s32[]{:T(128)}, ...), branch_computations={%region_1.0_spmd, %region_2.4_spmd} | conditional | flops 138020864 | bytes 4124758 | solution.py:135
  252.3 3.6 %conditional.3 = ((f32[512,1]{0,1:T(1,128)S(1)}, f32[512,1]{0,1:T(1,128)S(1)}, f32[512,1,128]{0,2,1:T(8,128)S(1)})) conditional(s32[]{:T(128)} %convert_element_type.116, (f32[512,1]{0,1:T(1,128)S(1)}, f32[512,1]{0,1:T(1,128)S(1)}, f32[512,1,128]{0,2,1:T(8,128)S(1)}) %tuple.60, (s32[]{:T(128)}, s32[512]{0:T(512)S(1)}, s32[]{:T(128)}, ...), branch_computations={%region_1.0_spmd, %region_2.4_spmd} | conditional | flops 138020864 | bytes 4124758 | solution.py:135
  273.3 3.7 %all-to-all-start = ((bf16[16,512,128]{2,1,0:T(8,128)(2,1)}), bf16[16,512,128]{2,1,0:T(8,128)(2,1)S(1)}, u32[]{:S(2)}, u32[]{:S(2)}) async-start(bf16[16,512,128]{2,1,0:T(8,128)(2,1)} %bitcast_bitcast_fusion), calls=%async_computation | async-start | bytes 4194304 | tf_op jit(solution)/shard_map/all_to_all | solution.py:24
  279.1 25.9 %all-to-all-done = bf16[16,512,128]{2,1,0:T(8,128)(2,1)S(1)} async-done(((bf16[16,512,128]{2,1,0:T(8,128)(2,1)}), bf16[16,512,128]{2,1,0:T(8,128)(2,1)S(1)}, u32[]{:S(2)}, u32[]{:S(2)}) %all-to-all-start) | async-done | bytes 2097184 | tf_op jit(solution)/shard_map/all_to_all | solution.py:24
  (371 shorter events, 212.0 us)
Async XLA Ops:
  7.2 79.2 %copy-start = (bf16[1,256,2048]{2,1,0:T(8,128)(2,1)S(1)}, bf16[1,256,2048]{2,1,0:T(8,128)(2,1)}, u32[]{:S(2)}) copy-start(bf16[1,256,2048]{2,1,0:T(8,128)(2,1)} %param.29) | copy-start | bytes 3145732
  7.2 6.6 %copy-start.4 = (s32[192,2]{0,1:T(2,128)S(1)}, s32[192,2]{0,1:T(2,128)}, u32[]{:S(2)}) copy-start(s32[192,2]{0,1:T(2,128)} %param.23) | copy-start | bytes 4612
  7.2 7.7 %copy-start.1 = (bf16[192,2048]{1,0:T(8,128)(2,1)S(1)}, bf16[192,2048]{1,0:T(8,128)(2,1)}, u32[]{:S(2)}) copy-start(bf16[192,2048]{1,0:T(8,128)(2,1)} %param.22) | copy-start | bytes 2359300
  7.2 6.6 %copy-start.5 = (f32[192,2]{0,1:T(2,128)S(1)}, f32[192,2]{0,1:T(2,128)}, u32[]{:S(2)}) copy-start(f32[192,2]{0,1:T(2,128)} %param.25) | copy-start | bytes 4612
  7.2 6.6 %copy-start.7 = (f32[192]{0:T(256)S(1)}, f32[192]{0:T(256)}, u32[]{:S(2)}) copy-start(f32[192]{0:T(256)} %param.24) | copy-start | bytes 2308
  7.2 139.6 %all-gather.2.cloned.1.call-start = ((), (), s32[]{:S(2)}) async-start(), calls=%async_computation.5 | async-start | bytes 8650752 | tf_op jit(solution)/shard_map/all_gather | solution.py:13
  81.8 3.3 %copy-start.2 = (bf16[32,18,2048]{2,1,0:T(8,128)(2,1)S(1)}, bf16[32,18,2048]{2,1,0:T(8,128)(2,1)}, u32[]{:S(2)}) copy-start(bf16[32,18,2048]{2,1,0:T(8,128)(2,1)} %reshape.213) | copy-start | bytes 7077892
  81.8 3.5 %copy-start.8 = (bf16[1,2048,256]{2,1,0:T(8,128)(2,1)S(1)}, bf16[1,2048,256]{2,1,0:T(8,128)(2,1)}, u32[]{:S(2)}) copy-start(bf16[1,2048,256]{2,1,0:T(8,128)(2,1)} %param.28) | copy-start | bytes 3145732
  96.4 31.4 %all-to-all-start.3 = ((bf16[16,576,128]{2,1,0:T(8,128)(2,1)}), bf16[16,576,128]{2,1,0:T(8,128)(2,1)S(1)}, u32[]{:S(2)}, u32[]{:S(2)}) async-start(bf16[16,576,128]{2,1,0:T(8,128)(2,1)} %copy.56), calls=%async_computation.3 | async-start | bytes 4718592 | tf_op jit(solution)/shard_map/all_to_all | solution.py:24
  128.8 144.5 %all-to-all-start.4 = ((bf16[32,18,128]{2,1,0:T(8,128)(2,1)}), bf16[32,18,128]{2,1,0:T(8,128)(2,1)S(1)}, u32[]{:S(2)}, u32[]{:S(2)}) async-start(bf16[32,18,128]{2,1,0:T(8,128)(2,1)} %all_to_all.31), calls=%async_computation.4 | async-start | bytes 393216 | tf_op jit(solution)/shard_map/all_to_all | solution.py:201
  146.8 5.8 %copy-start.6 = (f32[512,1]{0,1:T(1,128)S(1)}, f32[512,1]{0,1:T(1,128)}, u32[]{:S(2)}) copy-start(f32[512,1]{0,1:T(1,128)} %constant_dynamic-slice_fusion.1) | copy-start | bytes 6148
  146.8 5.8 %copy-start.9 = (bf16[512,128]{1,0:T(8,128)(2,1)S(1)}, bf16[512,128]{1,0:T(8,128)(2,1)}, u32[]{:S(2)}) copy-start(bf16[512,128]{1,0:T(8,128)(2,1)} %param.17) | copy-start | bytes 393220
  152.6 118.1 %copy-start.3 = (bf16[128,2048]{1,0:T(8,128)(2,1)S(1)}, bf16[128,2048]{1,0:T(8,128)(2,1)}, u32[]{:S(2)}) copy-start(bf16[128,2048]{1,0:T(8,128)(2,1)} %param.21) | copy-start | bytes 1572868
  273.3 31.7 %all-to-all-start = ((bf16[16,512,128]{2,1,0:T(8,128)(2,1)}), bf16[16,512,128]{2,1,0:T(8,128)(2,1)S(1)}, u32[]{:S(2)}, u32[]{:S(2)}) async-start(bf16[16,512,128]{2,1,0:T(8,128)(2,1)} %bitcast_bitcast_fusion), calls=%async_computation | async-start | bytes 4194304 | tf_op jit(solution)/shard_map/all_to_all | solution.py:24
Sparse Core Ops, SparseCore 0:
  10.2 84.1 all-gather.1
where the time goes:
time: 315 us; the launch traced here: 313 us
  matrix products  92.2 us (29%)
  blocking collectives  61.5 us (20%)
  waiting for transfers between devices  52.3 us (17%)
  local copies, waits for them, and re-layouts  48.5 us (15%)
  starting transfers between devices  25.4 us (8%)
  other arithmetic  15.4 us (5%)
  between operations  14.3 us (5%)
  loops' own time  3.22 us (1%)
    all_to_all x2, waiting for transfers between devices, sum_at_owner(): lax.all_to_all(tiles, axis, split_axis=0, concat_axis=0, tiled=True)  52.3 us
    dot_general x32, matrix products, attend_block(): jnp.einsum('qhk,khd->qhd', weights_now.astype(jnp.bfloat16), value_rows,...  42.5 us
    dot_general x32, matrix products, attend_block(): jnp.einsum('qhd,khd->qhk', queries_here, key_rows, preferred_element_type...  41.5 us
    all_to_all x1, blocking collectives, from_everyone(): return lax.all_to_all(copies, axis, split_axis=0, concat_axis=0, tiled=True)  36.3 us
    all_to_all x1, blocking collectives, body(): lax.all_to_all(outgoing, 'ep', split_axis=0, concat_axis=0, tiled=True)  25.2 us
    dynamic_slice x32, local copies, waits for them, and re-layouts, key_step(): lax.dynamic_slice_in_dim(log_gate_sums, key_offset, row_count, 0)  22.1 us
    all_to_all x1, starting transfers between devices, body(): lax.all_to_all(expert_out, 'ep', split_axis=0, concat_axis=0, tiled=True)  17.9 us
    reduce_sum x32, other arithmetic, attend_block(): weight_sum = weight_sum * shrink + jnp.sum(weights_now, axis=2)  7.68 us
  transfers between devices with their start and end apart: 4, of which 2 were waited for; matrix products, arithmetic and copies ran while one was open for 49% of the time, Pallas kernels for 0%

commit v1 on v0

v1 whole, which is shorter than its diff:
```python
import functools
import jax
import jax.numpy as jnp
from jax import lax
from jax.experimental import pallas as pl
from jax.experimental.pallas import tpu as pltpu
from jax.sharding import PartitionSpec as P

LOW_SCORE = -1e30
NORM_EPS = 1e-06
LOG2E = 1.4426950408889634
F32 = jnp.float32
BF16 = jnp.bfloat16


def nt_dot(a, b):
    return lax.dot_general(a, b, (((1,), (1,)), ((), ())), preferred_element_type=F32)


def nn_dot(a, b):
    return jnp.dot(a, b, preferred_element_type=F32)


def attention_kernel(
    index_ref, q_ref, gates_ref, kv_ref, mixer_ref, out_ref, m_ref, l_ref, acc_ref, *, chunk, per_block, sub
):
    step = pl.program_id(0)
    own = index_ref[0]
    rows, width = q_ref.shape
    scale = width ** (-0.5) * LOG2E

    @pl.when(step == 0)
    def _():
        m_ref[...] = jnp.full_like(m_ref, LOW_SCORE)
        l_ref[...] = jnp.zeros_like(l_ref)
        acc_ref[...] = jnp.zeros_like(acc_ref)

    def visit(j, masked):
        at = pl.ds(pl.multiple_of(j * chunk, chunk), chunk)
        k = kv_ref[at, :width]
        v = kv_ref[at, width:]
        gate = gates_ref[pl.ds(step * per_block + j, 1)].reshape(1, chunk)
        for r in range(0, rows, sub):
            rs = slice(r, r + sub)
            keys = chunk if not masked else min(chunk, r + sub)
            s = nt_dot(q_ref[rs], k[:keys]) * scale - gate[:, :keys]
            if masked:
                q_pos = lax.broadcasted_iota(jnp.int32, (sub, keys), 0) + r
                k_pos = lax.broadcasted_iota(jnp.int32, (sub, keys), 1)
                s = jnp.where(k_pos <= q_pos, s, LOW_SCORE)
            old = m_ref[rs]
            new = jnp.maximum(old, jnp.max(s, axis=1, keepdims=True))
            shrink = jnp.exp2(old - new)
            p = jnp.exp2(s - new[:, :1])
            part = p[:, :128]
            for c in range(128, keys, 128):
                part = part + p[:, c : c + 128]
            l_ref[rs] = l_ref[rs] * shrink + part
            acc_ref[rs] = acc_ref[rs] * shrink + nn_dot(p.astype(BF16), v[:keys])
            m_ref[rs] = new

    first = step * per_block
    full = jnp.clip(own - first, 0, per_block)

    def body(j, carry):
        visit(j, False)
        return carry

    lax.fori_loop(0, full, body, 0)

    @pl.when(own // per_block == step)
    def _():
        visit(own - first, True)

    @pl.when(step == pl.num_programs(0) - 1)
    def _():
        total = jnp.sum(l_ref[...], axis=1, keepdims=True)
        attended = (acc_ref[...] / total).astype(BF16)
        for t in range(out_ref.shape[0]):
            w = out_ref.shape[2]
            out_ref[t] = nn_dot(attended, mixer_ref[:, t * w : (t + 1) * w]).astype(BF16)


def attend(index, queries, gates, kv, mixer_weight, tp):
    rows, width = queries.shape
    length = kv.shape[0]
    per_block = 4
    blocks = length // rows // per_block
    spec = pltpu.PrefetchScalarGridSpec(
        num_scalar_prefetch=1,
        grid=(blocks,),
        in_specs=[
            pl.BlockSpec((rows, width), lambda b, i: (0, 0)),
            pl.BlockSpec(gates.shape, lambda b, i: (0, 0, 0)),
            pl.BlockSpec(
                (rows * per_block, 2 * width), lambda b, i: (jnp.minimum(b, i[0] // per_block), 0)
            ),
            pl.BlockSpec(mixer_weight.shape, lambda b, i: (0, 0)),
        ],
        out_specs=pl.BlockSpec((tp, rows, mixer_weight.shape[1] // tp), lambda b, i: (0, 0, 0)),
        scratch_shapes=[pltpu.VMEM((rows, 128), F32), pltpu.VMEM((rows, 128), F32), pltpu.VMEM((rows, width), F32)],
    )
    return pl.pallas_call(
        functools.partial(attention_kernel, chunk=rows, per_block=per_block, sub=SUB),
        out_shape=jax.ShapeDtypeStruct((tp, rows, mixer_weight.shape[1] // tp), BF16),
        grid_spec=spec,
        compiler_params=pltpu.CompilerParams(dimension_semantics=("arbitrary",)),
        cost_estimate=pl.CostEstimate(flops=8_000_000_000, bytes_accessed=12_000_000, transcendentals=8_000_000),
        name="attention",
    )(index, queries, gates, kv, mixer_weight)


SUB = 256


def experts_kernel(x_ref, gate_ref, up_ref, down_ref, out_ref, *, sub):
    tiles, rows, width = x_ref.shape
    for r in range(0, rows, sub):
        rs = slice(r, r + sub)
        x = jnp.concatenate([x_ref[t, rs] for t in range(tiles)], axis=1)
        g = nn_dot(x, gate_ref[0])
        u = nn_dot(x, up_ref[0])
        hidden = (g / (1.0 + jnp.exp(-g)) * u).astype(BF16)
        y = nn_dot(hidden, down_ref[0]).astype(BF16)
        for t in range(tiles):
            out_ref[t, rs] = y[:, t * width : (t + 1) * width]


def run_experts(x, gate_weight, up_weight, down_weight):
    return pl.pallas_call(
        functools.partial(experts_kernel, sub=192),
        out_shape=jax.ShapeDtypeStruct(x.shape, BF16),
        cost_estimate=pl.CostEstimate(flops=1_800_000_000, bytes_accessed=8_000_000, transcendentals=150_000),
        name="experts",
    )(x, gate_weight, up_weight, down_weight)


def route_kernel(index_ref, rows_ref, gain_ref, ids_ref, out_ref, slot_ref, *, experts, capacity):
    tokens, width = rows_ref.shape
    cols = out_ref.shape[1]
    x = rows_ref[...].astype(F32)
    inv = lax.rsqrt(jnp.mean(x * x, axis=1, keepdims=True) + NORM_EPS)
    at = pl.ds(pl.multiple_of(index_ref[0] * cols, cols), cols)
    own = (rows_ref[:, at].astype(F32) * inv * gain_ref[:, at]).astype(BF16)
    ids = ids_ref[...]
    expert = lax.broadcasted_iota(jnp.int32, (tokens, 128), 1)
    hits = [ids[:, k : k + 1] == expert for k in range(2)]
    both = jnp.where(hits[0] | hits[1], 1.0, 0.0).astype(BF16)
    row = lax.broadcasted_iota(jnp.int32, (tokens, tokens), 0)
    col = lax.broadcasted_iota(jnp.int32, (tokens, tokens), 1)
    earlier = nn_dot(jnp.where(col < row, 1.0, 0.0).astype(BF16), both)
    slots = []
    for k in range(2):
        rank = jnp.sum(jnp.where(hits[k], earlier, 0.0), axis=1, keepdims=True).astype(jnp.int32)
        slots.append(ids[:, k : k + 1] * capacity + rank)
    place = lax.broadcasted_iota(jnp.int32, (tokens, experts * capacity), 1)
    dispatch = jnp.where((place == slots[0]) | (place == slots[1]), 1.0, 0.0).astype(BF16)
    out_ref[...] = lax.dot_general(
        dispatch, own, (((0,), (0,)), ((), ())), preferred_element_type=F32
    ).astype(BF16)
    lane = lax.broadcasted_iota(jnp.int32, slot_ref.shape, 1)
    slot_ref[...] = jnp.where(lane == 0, slots[0], slots[1])


def route(index, rows, gain, ids, experts, capacity, cols):
    vmem = pl.BlockSpec(memory_space=pltpu.VMEM)
    return pl.pallas_call(
        functools.partial(route_kernel, experts=experts, capacity=capacity),
        out_shape=(
            jax.ShapeDtypeStruct((experts * capacity, cols), BF16),
            jax.ShapeDtypeStruct((rows.shape[0], 128), jnp.int32),
        ),
        in_specs=[pl.BlockSpec(memory_space=pltpu.SMEM), vmem, vmem, vmem],
        out_specs=(vmem, vmem),
        cost_estimate=pl.CostEstimate(flops=60_000_000, bytes_accessed=1_000_000, transcendentals=200),
        name="route",
    )(index, rows, gain, ids)


def combine_kernel(rows_ref, slot_ref, group_ref, inner_ref, out_ref):
    tokens = slot_ref.shape[0]
    inner = inner_ref[...]
    weight = group_ref[...] * inner / (inner[:, 0:1] + inner[:, 1:2])
    place = lax.broadcasted_iota(jnp.int32, (tokens, rows_ref.shape[0]), 1)
    total = 0.0
    for k in range(2):
        pick = jnp.where(place == slot_ref[:, k : k + 1], 1.0, 0.0).astype(BF16)
        total = total + weight[:, k : k + 1] * nn_dot(pick, rows_ref[...])
    out_ref[...] = total.astype(BF16)


def combine(rows, slots, group_gate, inner_gate):
    return pl.pallas_call(
        combine_kernel,
        out_shape=jax.ShapeDtypeStruct((slots.shape[0], rows.shape[1]), BF16),
        cost_estimate=pl.CostEstimate(flops=60_000_000, bytes_accessed=400_000, transcendentals=200),
        name="combine",
    )(rows, slots, group_gate, inner_gate)


def exchange(x, axis):
    return lax.all_to_all(x, axis, split_axis=0, concat_axis=0, tiled=True)


def summed(tiles):
    return tiles.astype(F32).sum(axis=0).astype(BF16)


def body(
    queries,
    keys,
    values,
    log_gate_sums,
    mixer_weight,
    moe_rows,
    route_ids,
    group_gate,
    inner_gate,
    norm_gain,
    gate_weight,
    up_weight,
    down_weight,
):
    rows = queries.shape[0]
    ep, tp = lax.axis_size("ep"), lax.axis_size("tp")
    ep_index = lax.axis_index("ep").astype(jnp.int32)
    tp_index = lax.axis_index("tp").astype(jnp.int32)
    kv = lax.all_gather(jnp.concatenate([keys, values], axis=1), "ep", axis=0, tiled=True)

    tokens, width = moe_rows.shape
    experts = ep * gate_weight.shape[0]
    capacity = 3 * tokens * route_ids.shape[1] // (2 * experts)
    cols = width // tp
    outgoing, slots = route(
        tp_index.reshape(1), moe_rows, norm_gain.reshape(1, -1), route_ids, experts, capacity, cols
    )
    arrived = exchange(outgoing.reshape(ep, capacity, cols), "ep").reshape(ep * capacity, cols)
    pieces = exchange(jnp.broadcast_to(arrived, (tp, *arrived.shape)), "tp")
    parts = run_experts(pieces, gate_weight, up_weight, down_weight)
    expert_out = summed(exchange(parts, "tp"))
    returned = exchange(expert_out.reshape(ep, capacity, cols), "ep").reshape(ep * capacity, cols)
    moe_out = combine(returned, slots, group_gate.reshape(-1, 1), inner_gate)

    start = lax.dynamic_slice_in_dim(log_gate_sums, ep_index * rows, 1, 0)
    gates = ((log_gate_sums - start) * LOG2E).reshape(ep, 1, rows)
    partial = attend(ep_index.reshape(1), queries, gates, kv, mixer_weight, tp)
    mixer_out = summed(exchange(partial, "tp"))
    return (mixer_out, moe_out)


def solution(mesh):
    return jax.shard_map(
        body,
        mesh=mesh,
        in_specs=(
            P("ep", "tp"),
            P("ep", "tp"),
            P("ep", "tp"),
            P(None, "tp"),
            P("tp", None),
            P("ep", None),
            P("ep", None),
            P("ep"),
            P("ep", None),
            P(),
            P("ep", None, "tp"),
            P("ep", None, "tp"),
            P("ep", "tp", None),
        ),
        out_specs=(P("ep", "tp"), P("ep", "tp")),
        check_vma=False,
    )
```

time: 315 us -> 227 us (0.72)
  matrix products: 92.2 us -> 0 us
  Pallas kernels: 0 us -> 47.6 us
  waiting for transfers between devices: 52.3 us -> 95.4 us
  local copies, waits for them, and re-layouts: 48.5 us -> 9.41 us
  blocking collectives: 61.5 us -> 25.2 us
  other arithmetic: 15.4 us -> 4.28 us
  starting transfers between devices: 25.4 us -> 30.2 us
  loops' own time: 3.22 us -> 0 us
    dot_general x70 -> x0, matrix products: 92.2 us -> none  [the longest x32 42.5 us: attend_block(): jnp.einsum('qhk,khd->qhd', weights_now.astype(jnp.bfloat16), value_rows,...]
    pallas_call x0 -> x4, Pallas kernels: none -> 47.6 us  [the longest x1 36.5 us: attend(): pl.pallas_call(functools.partial(attention_kernel, chunk=rows, per_block=...]
    all_to_all x3 -> x4, waiting for transfers between devices: 52.3 us -> 95.4 us  [exchange(): return lax.all_to_all(x, axis, split_axis=0, concat_axis=0, tiled=True)]
    all_to_all x2 -> x1, blocking collectives: 61.5 us -> 25.2 us  [exchange(): return lax.all_to_all(x, axis, split_axis=0, concat_axis=0, tiled=True)]
    dynamic_slice x34 -> x1, local copies, waits for them, and re-layouts: 24.1 us -> 0.56 us  [body(): start = lax.dynamic_slice_in_dim(log_gate_sums, ep_index * rows, 1, 0)]
    reduce_sum x38 -> x2, other arithmetic: 10.4 us -> 1.3 us  [summed(): return tiles.astype(F32).sum(axis=0).astype(BF16)]
    split x1 -> x0, local copies, waits for them, and re-layouts: 5.74 us -> none  [sent_together(): jnp.split(out, [sum(widths[:k]) for k in range(1, len(widths))], axis=along)]
    transpose x3 -> x0, local copies, waits for them, and re-layouts: 5.5 us -> none  [the longest x2 3.97 us: cut_along(): return jnp.moveaxis(x.reshape(*before, count, -1, *after), dim, 0)]
  transfers between devices with their start and end apart: 4 -> 5, of which waited for: 2 -> 3; matrix products, arithmetic and copies ran while one was open for 49% -> 4% of each run, Pallas kernels for 0% -> 21%
where the time goes in v1:
time: 227 us; the launch traced here: 226 us
  waiting for transfers between devices  95.4 us (42%)
  Pallas kernels  47.6 us (21%)
  starting transfers between devices  30.2 us (13%)
  blocking collectives  25.2 us (11%)
  between operations  14.1 us (6%)
  local copies, waits for them, and re-layouts  9.41 us (4%)
  other arithmetic  4.28 us (2%)
    all_to_all x4, waiting for transfers between devices, exchange(): return lax.all_to_all(x, axis, split_axis=0, concat_axis=0, tiled=True)  95.4 us
    pallas_call x1, Pallas kernels, attend(): pl.pallas_call(functools.partial(attention_kernel, chunk=rows, per_block=...  36.5 us
    all_to_all x4, starting transfers between devices, exchange(): return lax.all_to_all(x, axis, split_axis=0, concat_axis=0, tiled=True)  30.1 us
    all_to_all x1, blocking collectives, exchange(): return lax.all_to_all(x, axis, split_axis=0, concat_axis=0, tiled=True)  25.2 us
    pallas_call x1, Pallas kernels, run_experts(): pl.pallas_call(functools.partial(experts_kernel, sub=192), out_shape=jax....  6.41 us
  transfers between devices with their start and end apart: 5, of which 3 were waited for; matrix products, arithmetic and copies ran while one was open for 4% of the time, Pallas kernels for 21%

profile of v1, /device:TPU:481, one launch (start us, length us, event | category | flops | bytes accessed | tf_op | source)
XLA Modules:
  0.0 226.2 jit_solution(18117949495206852889)
XLA Ops:
  7.2 1.7 pad_maximum_fusion
  9.0 1.4 copy.17.ids_ref
  10.4 2.6 %route.1 = (bf16[576,128]{1,0:T(8,128)(2,1)}, s32[192,128]{1,0:T(8,128)}) custom-call(s32[1]{0:T(128)} %bitcast.3.index_ref, bf16[192,2048]{1,0:T(8,128)(2,1)} %rows_ref.1, f32[1,2048]{1,0:T(1,128)} %bitcast.7, s32[192,2]{1,0:T(8,128)} %copy.17.ids_ref), custom_call_target="tpu_custom_call" | custom-call | flops 60000000 | bytes 1000000 | tf_op jit(solution)/shard_map/route/pallas_call | solution.py:167
  13.0 1.0 reshape.37
  14.0 25.2 %all_to_all.25 = bf16[32,18,128]{2,1,0:T(8,128)(2,1)S(1)} all-to-all(bf16[32,18,128]{2,1,0:T(8,128)(2,1)S(1)} %reshape.37), channel_id=1, replica_groups=mesh['ep'=32,'tp'=16] {'ep'}, dimensions={0} | all-to-all | bytes 294912 | tf_op jit(solution)/shard_map/all_to_all | solution.py:202
  39.3 1.9 broadcast_in_dim.3
  41.2 7.2 %all-to-all-start.2 = ((bf16[16,576,128]{2,1,0:T(8,128)(2,1)}), bf16[16,576,128]{2,1,0:T(8,128)(2,1)S(1)}, u32[]{:S(2)}, u32[]{:S(2)}) async-start(bf16[16,576,128]{2,1,0:T(8,128)(2,1)} %broadcast_in_dim.3), calls=%async_computation.2 | async-start | bytes 4718592 | tf_op jit(solution)/shard_map/all_to_all | solution.py:202
  48.5 0.6 constant_dynamic-slice_fusion
  49.0 34.8 %all-to-all-done.2.x_ref = bf16[16,576,128]{2,1,0:T(8,128)(2,1)S(1)} async-done(((bf16[16,576,128]{2,1,0:T(8,128)(2,1)}), bf16[16,576,128]{2,1,0:T(8,128)(2,1)S(1)}, u32[]{:S(2)}, u32[]{:S(2)}) %all-to-all-start.2) | async-done | bytes 2359328 | tf_op jit(solution)/shard_map/all_to_all | solution.py:202
  83.8 1.5 copy-done
  85.3 6.4 %experts.1 = bf16[16,576,128]{2,1,0:T(8,128)(2,1)} custom-call(bf16[16,576,128]{2,1,0:T(8,128)(2,1)} %copy-done, bf16[1,2048,256]{2,1,0:T(8,128)(2,1)} %gate_ref.1, bf16[1,2048,256]{2,1,0:T(8,128)(2,1)} %up_ref.1, bf16[1,256,2048]{2,1,0:T(8,128)(2,1)} %down_ref.1), custom_call_target="tpu_custom_call" | custom-call | flops 1800000000 | bytes 8000000 | tf_op jit(solution)/shard_map/experts/pallas_call | solution.py:130
  91.7 3.7 %all-to-all-start.3 = ((bf16[16,576,128]{2,1,0:T(8,128)(2,1)}), bf16[16,576,128]{2,1,0:T(8,128)(2,1)S(1)}, u32[]{:S(2)}, u32[]{:S(2)}) async-start(bf16[16,576,128]{2,1,0:T(8,128)(2,1)} %experts.1), calls=%async_computation.3 | async-start | bytes 4718592 | tf_op jit(solution)/shard_map/all_to_all | solution.py:202
  95.4 1.3 subtract_multiply_fusion
  96.7 30.8 %all-to-all-done.3 = bf16[16,576,128]{2,1,0:T(8,128)(2,1)S(1)} async-done(((bf16[16,576,128]{2,1,0:T(8,128)(2,1)}), bf16[16,576,128]{2,1,0:T(8,128)(2,1)S(1)}, u32[]{:S(2)}, u32[]{:S(2)}) %all-to-all-start.3) | async-done | bytes 2359328 | tf_op jit(solution)/shard_map/all_to_all | solution.py:202
  127.8 0.7 reshape.39
  128.5 15.3 %all-to-all-start.4 = ((bf16[32,18,128]{2,1,0:T(8,128)(2,1)}), bf16[32,18,128]{2,1,0:T(8,128)(2,1)S(1)}, u32[]{:S(2)}, u32[]{:S(2)}) async-start(bf16[32,18,128]{2,1,0:T(8,128)(2,1)} %reshape.39), calls=%async_computation.4 | async-start | bytes 393216 | tf_op jit(solution)/shard_map/all_to_all | solution.py:202
  143.9 36.5 %attention.1 = bf16[16,512,128]{2,1,0:T(8,128)(2,1)} custom-call(s32[1]{0:T(128)} %bitcast.index_ref, bf16[512,128]{1,0:T(8,128)(2,1)} %q_ref.1, f32[32,1,512]{2,1,0:T(1,128)} %bitcast.6, bf16[16384,256]{1,0:T(8,128)(2,1)} %all-gather.2.cloned.1.call-done.kv_ref, bf16[128,2048]{1,0:T(8,128)(2,1)} %mixer_ref.1), custom_call_target="tpu_custom_call" | custom-call | flops 8000000000 | bytes 12000000 | tf_op jit(solution)/shard_map/attention/pallas_call | solution.py:103
  180.4 3.9 %all-to-all-start = ((bf16[16,512,128]{2,1,0:T(8,128)(2,1)}), bf16[16,512,128]{2,1,0:T(8,128)(2,1)S(1)}, u32[]{:S(2)}, u32[]{:S(2)}) async-start(bf16[16,512,128]{2,1,0:T(8,128)(2,1)} %attention.1), calls=%async_computation | async-start | bytes 4194304 | tf_op jit(solution)/shard_map/all_to_all | solution.py:202
  184.2 0.8 copy.18.group_ref
  185.0 0.8 copy.19.inner_ref
  185.8 0.7 reshape.40.rows_ref
  186.5 2.1 combine.1
  188.5 29.8 %all-to-all-done = bf16[16,512,128]{2,1,0:T(8,128)(2,1)S(1)} async-done(((bf16[16,512,128]{2,1,0:T(8,128)(2,1)}), bf16[16,512,128]{2,1,0:T(8,128)(2,1)S(1)}, u32[]{:S(2)}, u32[]{:S(2)}) %all-to-all-start) | async-done | bytes 2097184 | tf_op jit(solution)/shard_map/all_to_all | solution.py:202
  218.4 1.0 reduce_sum.24
  (13 shorter events, 0.5 us)
Async XLA Ops:
  7.2 136.7 %all-gather.2.cloned.1.call-start = ((), (), s32[]{:S(2)}) async-start(), calls=%async_computation.5 | async-start | bytes 8650752 | tf_op jit(solution)/shard_map/all_gather | solution.py:228
  41.2 7.2 %copy-start.1 = (f32[16384,1]{0,1:T(1,128)S(1)}, f32[16384,1]{0,1:T(1,128)}, u32[]{:S(2)}) copy-start(f32[16384,1]{0,1:T(1,128)} %param.16) | copy-start | bytes 196612
  41.2 42.6 %all-to-all-start.2 = ((bf16[16,576,128]{2,1,0:T(8,128)(2,1)}), bf16[16,576,128]{2,1,0:T(8,128)(2,1)S(1)}, u32[]{:S(2)}, u32[]{:S(2)}) async-start(bf16[16,576,128]{2,1,0:T(8,128)(2,1)} %broadcast_in_dim.3), calls=%async_computation.2 | async-start | bytes 4718592 | tf_op jit(solution)/shard_map/all_to_all | solution.py:202
  83.8 1.5 copy-start
  91.7 35.8 %all-to-all-start.3 = ((bf16[16,576,128]{2,1,0:T(8,128)(2,1)}), bf16[16,576,128]{2,1,0:T(8,128)(2,1)S(1)}, u32[]{:S(2)}, u32[]{:S(2)}) async-start(bf16[16,576,128]{2,1,0:T(8,128)(2,1)} %experts.1), calls=%async_computation.3 | async-start | bytes 4718592 | tf_op jit(solution)/shard_map/all_to_all | solution.py:202
  128.5 51.8 %all-to-all-start.4 = ((bf16[32,18,128]{2,1,0:T(8,128)(2,1)}), bf16[32,18,128]{2,1,0:T(8,128)(2,1)S(1)}, u32[]{:S(2)}, u32[]{:S(2)}) async-start(bf16[32,18,128]{2,1,0:T(8,128)(2,1)} %reshape.39), calls=%async_computation.4 | async-start | bytes 393216 | tf_op jit(solution)/shard_map/all_to_all | solution.py:202
  180.3 3.9 %copy-start.3 = (f32[192]{0:T(256)S(1)}, f32[192]{0:T(256)}, u32[]{:S(2)}) copy-start(f32[192]{0:T(256)} %param.20) | copy-start | bytes 2308
  180.3 4.7 %copy-start.2 = (f32[192,2]{0,1:T(2,128)S(1)}, f32[192,2]{0,1:T(2,128)}, u32[]{:S(2)}) copy-start(f32[192,2]{0,1:T(2,128)} %param.21) | copy-start | bytes 4612
  180.4 38.0 %all-to-all-start = ((bf16[16,512,128]{2,1,0:T(8,128)(2,1)}), bf16[16,512,128]{2,1,0:T(8,128)(2,1)S(1)}, u32[]{:S(2)}, u32[]{:S(2)}) async-start(bf16[16,512,128]{2,1,0:T(8,128)(2,1)} %attention.1), calls=%async_computation | async-start | bytes 4194304 | tf_op jit(solution)/shard_map/all_to_all | solution.py:202
Sparse Core Ops, SparseCore 0:
  10.1 82.5 all-gather.1
